TPU v7x, 256 devices: a whole 4x4x8 slice. The times are simulated.
256 devices in a mesh: ra: 32 (over z, y), cb: 8 (over x, core).
Axes of the slice: x: 4, y: 4, z: 8, core: 2. Of those that a mesh axis runs over, the one named last changes fastest.
Arguments:
- tokens: bfloat16 [2048, 16384], P('ra'), may hold values from -16 to 16
- norm_gain: float32 [2, 2048], replicated, may hold values from 0.1 to 1.9
- up_weight: float32 [2, 2048, 6144], P(None, 'ra', 'cb'), may hold values from -0.125 to 0.125
- gate_weight: float32 [2, 2048, 6144], P(None, 'ra', 'cb'), may hold values from -0.125 to 0.125
- up_scale: float32 [2, 6144], P(None, 'cb'), may hold values from 0.5 to 2
- gate_scale: float32 [2, 6144], P(None, 'cb'), may hold values from 0.5 to 2
- up_taps: float32 [2, 3, 6144], P(None, None, 'cb'), may hold values from -3 to 3
- gate_taps: float32 [2, 3, 6144], P(None, None, 'cb'), may hold values from -3 to 3
- down_weight: float32 [2, 2048, 6144], P(None, 'ra', 'cb'), may hold values from -0.078125 to 0.078125
- down_scale: float32 [2, 2048], replicated, may hold values from 0.5 to 2
Outputs:
- mixed: bfloat16 [2048, 16384], P('ra')
All inputs are finite; a program needn't handle non-finite values.
Results may differ from a plain program's by a relative error of at most 0.024.
Values may be sent and summed in bfloat16 or wider, within the bound.
No kernel may reach another device: no remote copies, remote signals or barrier semaphores. Data moves between devices by JAX's collectives and lax.ppermute only.
A program may use at most 64 MiB of HBM per device.

v0:
```python
import jax
import jax.numpy as jnp
from jax import lax
from jax.sharding import Mesh
from jax.sharding import PartitionSpec as P

RA = ("ra_0", "ra_1")
EPS = 1e-06
RESIDUAL = 0.5


def shifted(value, axis, steps):
    count = lax.axis_size(axis)
    initial, last = (max(0, -steps), min(count, count - steps))
    return lax.ppermute(value, axis, [(source, source + steps) for source in range(initial, last)])


def sent_together(arrays, axis, dim, along):
    ends, at = ([], 0)
    for a in arrays[:-1]:
        at += a.shape[along]
        ends.append(at)
    both = jnp.concatenate(arrays, axis=along)
    return tuple(jnp.split(lax.all_gather(both, axis, axis=dim, tiled=True), ends, axis=along))


def gather_axes(value, axes, dim):
    whole = value
    for number in range(len(axes) - 1, -1, -1):
        whole = lax.all_gather(whole, axes[number], axis=dim, tiled=True)
    return whole


def padded_to(lines, length):
    spare = -len(lines) % length
    return jnp.pad(lines, [(0, spare)] + [(0, 0)] * (lines.ndim - 1))


def total_of(value, axis):
    lines = value.reshape(-1, *value.shape[1:][-1:])
    own = lax.psum_scatter(
        padded_to(lines, lax.axis_size(axis)), axis, scatter_dimension=0, tiled=True
    )
    whole = lax.all_gather(own, axis).reshape(-1, *lines.shape[1:])
    return lax.slice_in_dim(whole, 0, len(lines)).reshape(value.shape)


def valid_taps(values, taps):
    width = taps.shape[0]
    length = values.shape[0] - width + 1
    total = taps[0][None, :] * values[0:length]
    for k in range(1, width):
        total = total + taps[k][None, :] * values[k : k + length]
    return total


def per_device(
    tokens,
    norm_gain,
    up_weight,
    gate_weight,
    up_scale,
    gate_scale,
    up_taps,
    gate_taps,
    down_weight,
    down_scale,
):
    state = lax.all_to_all(tokens, RA, split_axis=1, concat_axis=0, tiled=True).T
    edge = up_taps.shape[1] - 1
    for layer in range(up_weight.shape[0]):
        before = shifted(state[state.shape[0] - edge :], RA, 1)
        rows = jnp.concatenate([before, state], axis=0)
        rows_f = rows.astype(jnp.float32)
        inverse = lax.rsqrt(jnp.mean(rows_f * rows_f, axis=1, keepdims=True) + EPS)
        scaled = (rows_f * norm_gain[layer][None, :]).astype(jnp.bfloat16)
        pieces = sent_together(
            (up_weight[layer].astype(jnp.bfloat16), gate_weight[layer].astype(jnp.bfloat16)),
            RA,
            0,
            1,
        )
        up_raw = jnp.dot(scaled, pieces[0], preferred_element_type=jnp.float32)
        gate_raw = jnp.dot(scaled, pieces[1], preferred_element_type=jnp.float32)
        up_pre = up_raw * inverse * up_scale[layer][None, :]
        gate_pre = gate_raw * inverse * gate_scale[layer][None, :]
        conv_up = valid_taps(up_pre, up_taps[layer])
        conv_gate = valid_taps(gate_pre, gate_taps[layer])
        hidden = (jax.nn.silu(conv_gate) * conv_up).astype(jnp.bfloat16)
        down_part = lax.dot_general(
            hidden,
            gather_axes(down_weight[layer].astype(jnp.bfloat16), RA, 0),
            (((1,), (1,)), ((), ())),
            preferred_element_type=jnp.float32,
        )
        down = total_of(down_part.astype(jnp.bfloat16), "cb").astype(jnp.float32)
        state = (down * down_scale[layer][None, :] + RESIDUAL * state.astype(jnp.float32)).astype(
            jnp.bfloat16
        )
    return lax.all_to_all(state.T, RA, split_axis=0, concat_axis=1, tiled=True)


def solution(mesh):
    torus = Mesh(mesh.devices.reshape(8, 4, mesh.shape["cb"]), ("ra_0", "ra_1", "cb"))
    placed = (
        P(RA, None),
        P(),
        P(None, RA, "cb"),
        P(None, RA, "cb"),
        P(None, "cb"),
        P(None, "cb"),
        P(None, None, "cb"),
        P(None, None, "cb"),
        P(None, RA, "cb"),
        P(),
    )
    return jax.shard_map(
        per_device, mesh=torus, in_specs=placed, out_specs=P(RA, None), check_vma=False
    )
```

profile of v0, /device:TPU:8, one launch (start us, length us, event | category | flops | bytes accessed | tf_op | source)
XLA Modules:
  0.0 512.2 jit_solution(13660260227973896724)
XLA Ops:
  11.1 11.8 %all-to-all-start = ((bf16[64,32,512]{2,0,1:T(8,128)(2,1)}), bf16[64,32,512]{2,0,1:T(8,128)(2,1)S(1)}, u32[]{:S(2)}, u32[]{:S(2)}) async-start(bf16[64,32,512]{2,0,1:T(8,128)(2,1)} %bitcast.42), calls=%async_computation | async-start | bytes 4194304 | tf_op jit(solution)/shard_map/all_to_all | solution.py:69
  23.1 19.1 %all-gather = bf16[1,256,768]{2,1,0:T(8,128)(2,1)} all-gather(bf16[1,64,768]{2,1,0:T(8,128)(2,1)S(1)} %get-tuple-element.26), channel_id=2, replica_groups=mesh['ra_0'=8,'ra_1'=4,'cb'=8] {'ra_1'}, dimensions={1}, use_global_device_ids=true | all-gather | bytes 491520 | tf_op jit(solution)/shard_map/all_gather | solution.py:30
  42.5 37.1 %all-to-all-done = bf16[64,32,512]{2,0,1:T(8,128)(2,1)S(1)} async-done(((bf16[64,32,512]{2,0,1:T(8,128)(2,1)}), bf16[64,32,512]{2,0,1:T(8,128)(2,1)S(1)}, u32[]{:S(2)}, u32[]{:S(2)}) %all-to-all-start) | async-done | bytes 2097184 | tf_op jit(solution)/shard_map/all_to_all | solution.py:69
  80.9 3.0 copy.20
  83.9 3.9 collective-permute-start
  90.6 20.9 %all-gather.13.cloned.1.call-done = bf16[2048,1536]{1,0:T(8,128)(2,1)} async-done(((bf16[64,1536]{1,0:T(8,128)(2,1)}), bf16[2048,1536]{1,0:T(8,128)(2,1)}) %all-gather.13.cloned.1.call-update) | async-done | bytes 6291472 | tf_op jit(solution)/shard_map/all_gather | solution.py:24
  111.5 5.2 %multiply_multiply_fusion.3 = f32[514,768]{1,0:T(8,128)} fusion(bf16[2048,1536]{1,0:T(8,128)(2,1)} %all-gather.13.cloned.1.call-done, f32[2048]{0:T(1024)S(1)} %bitcast.50, f32[768]{0:T(1024)S(1)} %get-tuple-element.18, f32[514]{0:T(1024)S(1)} %add_rsqrt_fusion.1, bf16[512,2048]{1,0:T(8,128)(2,1)S(1)} %bitcast.39, bf16[2,2048]{1,0:T(2,128)(2,1)S(1)} %collective-permute-done), kind=kOutput, calls=%fused_computation.35 | convolution fusion | flops 1624009728 | bytes 6843400 | tf_op jit(solution)/shard_map/dot_general | solution.py:84
  116.7 3.1 multiply_multiply_fusion.2
  119.8 36.8 %all-gather.17.cloned.1.call-done = bf16[1,2048,768]{2,1,0:T(8,128)(2,1)} async-done(((bf16[1,256,768]{2,1,0:T(8,128)(2,1)}), bf16[1,2048,768]{2,1,0:T(8,128)(2,1)}) %all-gather.17.cloned.1.call-update) | async-done | bytes 3145744 | tf_op jit(solution)/shard_map/all_gather | solution.py:30
  156.5 8.9 %fusion.20 = bf16[512,2048]{1,0:T(8,128)(2,1)} fusion(bf16[1,2048,768]{2,1,0:T(8,128)(2,1)} %all-gather.17.cloned.1.call-done, f32[514,768]{1,0:T(8,128)} %multiply_multiply_fusion.2, f32[514,768]{1,0:T(8,128)} %multiply_multiply_fusion.3, f32[768]{0:T(1024)S(1)} %get-tuple-element.12, f32[768]{0:T(1024)S(1)} %get-tuple-element.13, ...), kind=kOutput, calls=%fused_computation.26 | convolution fusion | flops 1617952768 | bytes 14698496 | tf_op jit(solution)/shard_map/dot_general | solution.py:90
  165.5 35.1 %reduce-scatter.3.cloned.1.call-done = bf16[64,2048]{1,0:T(8,128)(2,1)} async-done(((bf16[512,2048]{1,0:T(8,128)(2,1)}), bf16[64,2048]{1,0:T(8,128)(2,1)}) %reduce-scatter.3.cloned.1.call-update) | async-done | bytes 262160 | tf_op jit(solution)/shard_map/reduce_scatter | solution.py:41
  201.4 13.3 %all-gather.3 = bf16[1,256,768]{2,1,0:T(8,128)(2,1)} all-gather(bf16[1,64,768]{2,1,0:T(8,128)(2,1)S(1)} %get-tuple-element.25), channel_id=5, replica_groups=mesh['ra_0'=8,'ra_1'=4,'cb'=8] {'ra_1'}, dimensions={1}, use_global_device_ids=true | all-gather | bytes 491520 | tf_op jit(solution)/shard_map/all_gather | solution.py:30
  214.8 14.2 %all-gather.19.cloned.1.call-done = bf16[512,2048]{1,0:T(8,128)(2,1)} async-done(((bf16[64,2048]{1,0:T(8,128)(2,1)}), bf16[512,2048]{1,0:T(8,128)(2,1)}) %all-gather.19.cloned.1.call-update) | async-done | bytes 2097168 | tf_op jit(solution)/shard_map/all_gather | solution.py:44
  231.5 3.6 collective-permute-start.1
  237.9 80.9 %all-gather.15.cloned.1.call-done = bf16[2048,1536]{1,0:T(8,128)(2,1)} async-done(((bf16[64,1536]{1,0:T(8,128)(2,1)}), bf16[2048,1536]{1,0:T(8,128)(2,1)}) %all-gather.15.cloned.1.call-update) | async-done | bytes 6291472 | tf_op jit(solution)/shard_map/all_gather | solution.py:24
  318.8 5.8 %multiply_multiply_fusion.1 = f32[514,768]{1,0:T(8,128)} fusion(bf16[2048,1536]{1,0:T(8,128)(2,1)} %all-gather.15.cloned.1.call-done, f32[2048]{0:T(1024)S(1)} %bitcast.48, f32[768]{0:T(1024)S(1)} %get-tuple-element.17, f32[514]{0:T(1024)S(1)} %add_rsqrt_fusion, bf16[512,2048]{1,0:T(8,128)(2,1)} %copy-done, bf16[2,2048]{1,0:T(2,128)(2,1)S(1)} %collective-permute-done.1), kind=kOutput, calls=%fused_computation.33 | convolution fusion | flops 1624009728 | bytes 6843400 | tf_op jit(solution)/shard_map/dot_general | solution.py:84
  324.6 3.1 multiply_multiply_fusion
  327.7 36.0 %all-gather.21.cloned.1.call-done = bf16[1,2048,768]{2,1,0:T(8,128)(2,1)} async-done(((bf16[1,256,768]{2,1,0:T(8,128)(2,1)}), bf16[1,2048,768]{2,1,0:T(8,128)(2,1)}) %all-gather.21.cloned.1.call-update) | async-done | bytes 3145744 | tf_op jit(solution)/shard_map/all_gather | solution.py:30
  363.7 8.9 %fusion.23 = bf16[512,2048]{1,0:T(8,128)(2,1)} fusion(bf16[1,2048,768]{2,1,0:T(8,128)(2,1)} %all-gather.21.cloned.1.call-done, f32[514,768]{1,0:T(8,128)} %multiply_multiply_fusion, f32[514,768]{1,0:T(8,128)} %multiply_multiply_fusion.1, f32[768]{0:T(1024)S(1)} %get-tuple-element.15, f32[768]{0:T(1024)S(1)} %get-tuple-element.16, ...), kind=kOutput, calls=%fused_computation.27 | convolution fusion | flops 1617952768 | bytes 14698496 | tf_op jit(solution)/shard_map/dot_general | solution.py:90
  372.6 35.1 %reduce-scatter.5.cloned.1.call-done = bf16[64,2048]{1,0:T(8,128)(2,1)} async-done(((bf16[512,2048]{1,0:T(8,128)(2,1)}), bf16[64,2048]{1,0:T(8,128)(2,1)}) %reduce-scatter.5.cloned.1.call-update) | async-done | bytes 262160 | tf_op jit(solution)/shard_map/reduce_scatter | solution.py:41
  407.7 28.6 %all-gather.23.cloned.1.call-done = bf16[512,2048]{1,0:T(8,128)(2,1)} async-done(((bf16[64,2048]{1,0:T(8,128)(2,1)}), bf16[512,2048]{1,0:T(8,128)(2,1)}) %all-gather.23.cloned.1.call-update) | async-done | bytes 2097168 | tf_op jit(solution)/shard_map/all_gather | solution.py:44
  436.3 3.8 fusion.26
  440.1 2.9 copy.21
  443.0 60.9 %all_to_all.38 = bf16[32,64,512]{2,1,0:T(8,128)(2,1)S(1)} all-to-all(bf16[32,64,512]{2,1,0:T(8,128)(2,1)S(1)} %bitcast.43), channel_id=1, replica_groups=mesh['ra_0'=8,'ra_1'=4,'cb'=8] {'ra_0','ra_1'}, dimensions={0} | all-to-all | bytes 4194304 | tf_op jit(solution)/shard_map/all_to_all | solution.py:100
  (65 shorter events, 16.7 us)
Async XLA Ops:
  6.5 3.0 copy-start.3
  6.5 105.0 %all-gather.13.cloned.1.call-start = ((), (), s32[]{:S(2)}) async-start(), calls=%async_computation.4 | async-start | bytes 6488064 | tf_op jit(solution)/shard_map/all_gather | solution.py:24
  11.1 11.9 %copy-start.4 = (f32[2,64,768]{2,1,0:T(8,128)S(1)}, f32[2,64,768]{2,1,0:T(8,128)}, u32[]{:S(2)}) copy-start(f32[2,64,768]{2,1,0:T(8,128)} %param.18) | copy-start | bytes 1179652
  11.1 31.2 %copy-start.9 = (f32[2,768]{1,0:T(2,128)S(1)}, f32[2,768]{1,0:T(2,128)}, u32[]{:S(2)}) copy-start(f32[2,768]{1,0:T(2,128)} %param.15) | copy-start | bytes 18436
  11.1 31.2 %copy-start.5 = (f32[2,3,768]{2,0,1:T(2,128)S(1)}, f32[2,3,768]{2,0,1:T(2,128)}, u32[]{:S(2)}) copy-start(f32[2,3,768]{2,0,1:T(2,128)} %param.16) | copy-start | bytes 55300
  11.1 31.2 %copy-start.6 = (f32[2,3,768]{2,0,1:T(2,128)S(1)}, f32[2,3,768]{2,0,1:T(2,128)}, u32[]{:S(2)}) copy-start(f32[2,3,768]{2,0,1:T(2,128)} %param.17) | copy-start | bytes 55300
  11.1 31.4 %copy-start.7 = (f32[2,2048]{1,0:T(2,128)S(1)}, f32[2,2048]{1,0:T(2,128)}, u32[]{:S(2)}) copy-start(f32[2,2048]{1,0:T(2,128)} %param.11) | copy-start | bytes 49156
  11.1 68.5 %all-to-all-start = ((bf16[64,32,512]{2,0,1:T(8,128)(2,1)}), bf16[64,32,512]{2,0,1:T(8,128)(2,1)S(1)}, u32[]{:S(2)}, u32[]{:S(2)}) async-start(bf16[64,32,512]{2,0,1:T(8,128)(2,1)} %bitcast.42), calls=%async_computation | async-start | bytes 4194304 | tf_op jit(solution)/shard_map/all_to_all | solution.py:69
  23.0 133.5 %all-gather.17.cloned.1.call-start = ((), (), s32[]{:S(2)}) async-start(), calls=%async_computation.8 | async-start | bytes 3538944 | tf_op jit(solution)/shard_map/all_gather | solution.py:30
  42.3 158.3 %reduce-scatter.3.cloned.1.call-start = ((), (), s32[]{:S(2)}) async-start(), calls=%async_computation.5 | async-start | bytes 2359296 | tf_op jit(solution)/shard_map/reduce_scatter | solution.py:41
  79.6 1.3 copy-start.2
  80.9 6.9 %copy-start.10 = (f32[2,768]{1,0:T(2,128)S(1)}, f32[2,768]{1,0:T(2,128)}, u32[]{:S(2)}) copy-start(f32[2,768]{1,0:T(2,128)} %param.14) | copy-start | bytes 18436
  83.9 5.8 %collective-permute-start = (bf16[2,2048]{1,0:T(2,128)(2,1)S(1)}, bf16[2,2048]{1,0:T(2,128)(2,1)S(1)}, u32[]{:S(2)}, u32[]{:S(2)}) collective-permute-start(bf16[2,2048]{1,0:T(2,128)(2,1)S(1)} %slice.194), channel_id=1, source_target_pairs={{0,8},{8,16},{16,24},{24,32},{32,40},{40,48},{48,56},{56,64},{64,7... | collective-permute-start | bytes 24584 | tf_op jit(solution)/shard_map/ppermute | solution.py:15
  111.5 5.2 %copy-start.11 = (bf16[2048,1536]{1,0:T(8,128)(2,1)S(1)}, bf16[2048,1536]{1,0:T(8,128)(2,1)}, u32[]{:S(2)}) copy-start(bf16[2048,1536]{1,0:T(8,128)(2,1)} %all-gather.13.cloned.1.call-done) | copy-start | bytes 18874372
  165.4 49.4 %copy-start.8 = (f32[2,2048]{1,0:T(2,128)S(1)}, f32[2,2048]{1,0:T(2,128)}, u32[]{:S(2)}) copy-start(f32[2,2048]{1,0:T(2,128)} %param.19) | copy-start | bytes 49156
  165.5 63.6 %all-gather.19.cloned.1.call-start = ((), (), s32[]{:S(2)}) async-start(), calls=%async_computation.9 | async-start | bytes 2359296 | tf_op jit(solution)/shard_map/all_gather | solution.py:44
  200.6 118.2 %all-gather.15.cloned.1.call-start = ((), (), s32[]{:S(2)}) async-start(), calls=%async_computation.6 | async-start | bytes 6488064 | tf_op jit(solution)/shard_map/all_gather | solution.py:24
  201.4 162.3 %all-gather.21.cloned.1.call-start = ((), (), s32[]{:S(2)}) async-start(), calls=%async_computation.10 | async-start | bytes 3538944 | tf_op jit(solution)/shard_map/all_gather | solution.py:30
  214.7 193.0 %reduce-scatter.5.cloned.1.call-start = ((), (), s32[]{:S(2)}) async-start(), calls=%async_computation.7 | async-start | bytes 2359296 | tf_op jit(solution)/shard_map/reduce_scatter | solution.py:41
  231.5 5.6 %copy-start = (bf16[512,2048]{1,0:T(8,128)(2,1)}, bf16[512,2048]{1,0:T(8,128)(2,1)S(1)}, u32[]{:S(2)}) copy-start(bf16[512,2048]{1,0:T(8,128)(2,1)S(1)} %fusion.7) | copy-start | bytes 6291460
  231.5 5.5 %collective-permute-start.1 = (bf16[2,2048]{1,0:T(2,128)(2,1)S(1)}, bf16[2,2048]{1,0:T(2,128)(2,1)S(1)}, u32[]{:S(2)}, u32[]{:S(2)}) collective-permute-start(bf16[2,2048]{1,0:T(2,128)(2,1)S(1)} %slice.204), channel_id=1, source_target_pairs={{0,8},{8,16},{16,24},{24,32},{32,40},{40,48},{48,56},{56,64},{64,7... | collective-permute-start | bytes 24584 | tf_op jit(solution)/shard_map/ppermute | solution.py:15
  318.8 5.8 %copy-start.1 = (bf16[512,2048]{1,0:T(8,128)(2,1)S(1)}, bf16[512,2048]{1,0:T(8,128)(2,1)}, u32[]{:S(2)}) copy-start(bf16[512,2048]{1,0:T(8,128)(2,1)} %copy-done) | copy-start | bytes 6291460
  318.8 5.8 %copy-start.12 = (bf16[2048,1536]{1,0:T(8,128)(2,1)S(1)}, bf16[2048,1536]{1,0:T(8,128)(2,1)}, u32[]{:S(2)}) copy-start(bf16[2048,1536]{1,0:T(8,128)(2,1)} %all-gather.15.cloned.1.call-done) | copy-start | bytes 18874372
  372.6 63.7 %all-gather.23.cloned.1.call-start = ((), (), s32[]{:S(2)}) async-start(), calls=%async_computation.11 | async-start | bytes 2359296 | tf_op jit(solution)/shard_map/all_gather | solution.py:44
Sparse Core Ops, SparseCore 0:
  9.9 101.5 all-gather.12
  113.3 43.1 all-gather.16
  165.6 34.9 reduce-scatter.2
  202.3 26.6 all-gather.18
  231.4 87.3 all-gather.14
  320.5 43.1 all-gather.20
  372.7 34.9 reduce-scatter.4
  409.6 26.6 all-gather.22
where the time goes:
time: 513 us; the launch traced here: 512 us
  waiting for transfers between devices  328 us (64%)
  blocking collectives  93.3 us (18%)
  matrix products  34.9 us (7%)
  starting transfers between devices  19.6 us (4%)
  between operations  13.7 us (3%)
  other arithmetic  11.6 us (2%)
  local copies, waits for them, and re-layouts  10.6 us (2%)
    all_gather x2, waiting for transfers between devices, sent_together(): lax.all_gather(both, axis, axis=dim, tiled=True)  102 us
    all_gather x2, waiting for transfers between devices, gather_axes(): whole = lax.all_gather(whole, axes[number], axis=dim, tiled=True)  72.7 us
    reduce_scatter x2, waiting for transfers between devices, total_of(): lax.psum_scatter(padded_to(lines, lax.axis_size(axis)), axis, scatter_dim...  70.1 us
    all_to_all x1, blocking collectives, per_device(): return lax.all_to_all(state.T, RA, split_axis=0, concat_axis=1, tiled=True)  60.9 us
    all_gather x2, waiting for transfers between devices, total_of(): whole = lax.all_gather(own, axis).reshape(-1, *lines.shape[1:])  42.7 us
    all_to_all x1, waiting for transfers between devices, per_device(): lax.all_to_all(tokens, RA, split_axis=1, concat_axis=0, tiled=True)  37.1 us
    all_gather x2, blocking collectives, gather_axes(): whole = lax.all_gather(whole, axes[number], axis=dim, tiled=True)  32.4 us
    dot_general x2, matrix products, per_device(): lax.dot_general(hidden, gather_axes(down_weight[layer].astype(jnp.bfloat1...  17.8 us
  transfers between devices with their start and end apart: 11, of which 11 were waited for; matrix products, arithmetic and copies ran while one was open for 5% of the time, Pallas kernels for 0%

commit v1 on v0

--- a/solution.py
+++ b/solution.py
@@ -66,7 +66,9 @@
     down_weight,
     down_scale,
 ):
-    state = lax.all_to_all(tokens, RA, split_axis=1, concat_axis=0, tiled=True).T
+    state = jnp.concatenate(
+        lax.all_to_all(jnp.stack(jnp.split(tokens, lax.axis_size(RA), axis=1)), RA, 0, 0), axis=0
+    ).T
     edge = up_taps.shape[1] - 1
     for layer in range(up_weight.shape[0]):
         before = shifted(state[state.shape[0] - edge :], RA, 1)

time: 513 us -> 524 us (1.021)
  local copies, waits for them, and re-layouts: 10.6 us -> 29.2 us
    unnamed x26 -> x57, local copies, waits for them, and re-layouts: 1.37 us -> 21 us
    all_gather x2, waiting for transfers between devices: 102 us -> 87.2 us  [sent_together(): lax.all_gather(both, axis, axis=dim, tiled=True)]
    all_to_all x1, waiting for transfers between devices: 37.1 us -> 48.2 us  [per_device(): lax.all_to_all(jnp.stack(jnp.split(tokens, lax.axis_size(RA), axis=1)), R...]
  transfers between devices with their start and end apart: 11 -> 11, of which waited for: 11 -> 11; matrix products, arithmetic and copies ran while one was open for 5% -> 9% of each run, Pallas kernels for 0% -> 0%
where the time goes in v1:
time: 524 us; the launch traced here: 523 us
  waiting for transfers between devices  325 us (62%)
  blocking collectives  88.7 us (17%)
  matrix products  34.9 us (7%)
  local copies, waits for them, and re-layouts  29.2 us (6%)
  starting transfers between devices  19.6 us (4%)
  between operations  13.7 us (3%)
  other arithmetic  11.6 us (2%)
    all_gather x2, waiting for transfers between devices, sent_together(): lax.all_gather(both, axis, axis=dim, tiled=True)  87.2 us
    all_gather x2, waiting for transfers between devices, gather_axes(): whole = lax.all_gather(whole, axes[number], axis=dim, tiled=True)  73.4 us
    reduce_scatter x2, waiting for transfers between devices, total_of(): lax.psum_scatter(padded_to(lines, lax.axis_size(axis)), axis, scatter_dim...  70.1 us
    all_to_all x1, blocking collectives, per_device(): return lax.all_to_all(state.T, RA, split_axis=0, concat_axis=1, tiled=True)  60.9 us
    all_to_all x1, waiting for transfers between devices, per_device(): lax.all_to_all(jnp.stack(jnp.split(tokens, lax.axis_size(RA), axis=1)), R...  48.2 us
    all_gather x2, waiting for transfers between devices, total_of(): whole = lax.all_gather(own, axis).reshape(-1, *lines.shape[1:])  42.7 us
    all_gather x2, blocking collectives, gather_axes(): whole = lax.all_gather(whole, axes[number], axis=dim, tiled=True)  27.9 us
    unnamed x57, local copies, waits for them, and re-layouts  21 us
  transfers between devices with their start and end apart: 11, of which 11 were waited for; matrix products, arithmetic and copies ran while one was open for 9% of the time, Pallas kernels for 0%

profile of v1, /device:TPU:8, one launch (start us, length us, event | category | flops | bytes accessed | tf_op | source)
XLA Modules:
  0.0 523.1 jit_solution(11889408912213434894)
XLA Ops:
  29.8 11.8 %all-to-all-start = ((bf16[32,64,512]{2,1,0:T(8,128)(2,1)}), bf16[32,64,512]{2,1,0:T(8,128)(2,1)S(1)}, u32[]{:S(2)}, u32[]{:S(2)}) async-start(bf16[32,64,512]{2,1,0:T(8,128)(2,1)} %constant_dynamic-update-slice_fusion), calls=%async_computation | async-start | bytes 4194304 | tf_op jit(solution)/shard_map/all_to_all | solution.py:70
  41.8 14.6 %all-gather = bf16[1,256,768]{2,1,0:T(8,128)(2,1)} all-gather(bf16[1,64,768]{2,1,0:T(8,128)(2,1)S(1)} %get-tuple-element.26), channel_id=2, replica_groups=mesh['ra_0'=8,'ra_1'=4,'cb'=8] {'ra_1'}, dimensions={1}, use_global_device_ids=true | all-gather | bytes 491520 | tf_op jit(solution)/shard_map/all_gather | solution.py:30
  56.6 48.2 %all-to-all-done = bf16[32,64,512]{2,1,0:T(8,128)(2,1)S(1)} async-done(((bf16[32,64,512]{2,1,0:T(8,128)(2,1)}), bf16[32,64,512]{2,1,0:T(8,128)(2,1)S(1)}, u32[]{:S(2)}, u32[]{:S(2)}) %all-to-all-start) | async-done | bytes 2097184 | tf_op jit(solution)/shard_map/all_to_all | solution.py:70
  106.1 2.9 copy.15
  109.1 3.9 collective-permute-start
  115.5 6.3 %all-gather.13.cloned.1.call-done = bf16[2048,1536]{1,0:T(8,128)(2,1)} async-done(((bf16[64,1536]{1,0:T(8,128)(2,1)}), bf16[2048,1536]{1,0:T(8,128)(2,1)}) %all-gather.13.cloned.1.call-update) | async-done | bytes 6291472 | tf_op jit(solution)/shard_map/all_gather | solution.py:24
  121.7 5.2 multiply_multiply_fusion.3
  126.9 3.1 multiply_multiply_fusion.2
  130.0 37.4 %all-gather.17.cloned.1.call-done = bf16[1,2048,768]{2,1,0:T(8,128)(2,1)} async-done(((bf16[1,256,768]{2,1,0:T(8,128)(2,1)}), bf16[1,2048,768]{2,1,0:T(8,128)(2,1)}) %all-gather.17.cloned.1.call-update) | async-done | bytes 3145744 | tf_op jit(solution)/shard_map/all_gather | solution.py:30
  167.4 8.9 %fusion.20 = bf16[512,2048]{1,0:T(8,128)(2,1)} fusion(bf16[1,2048,768]{2,1,0:T(8,128)(2,1)} %all-gather.17.cloned.1.call-done, f32[514,768]{1,0:T(8,128)} %multiply_multiply_fusion.2, f32[514,768]{1,0:T(8,128)} %multiply_multiply_fusion.3, f32[768]{0:T(1024)S(1)} %get-tuple-element.12, f32[768]{0:T(1024)S(1)} %get-tuple-element.13, ...), kind=kOutput, calls=%fused_computation.26 | convolution fusion | flops 1617952768 | bytes 14698496 | tf_op jit(solution)/shard_map/dot_general | solution.py:92
  176.4 35.1 %reduce-scatter.3.cloned.1.call-done = bf16[64,2048]{1,0:T(8,128)(2,1)} async-done(((bf16[512,2048]{1,0:T(8,128)(2,1)}), bf16[64,2048]{1,0:T(8,128)(2,1)}) %reduce-scatter.3.cloned.1.call-update) | async-done | bytes 262160 | tf_op jit(solution)/shard_map/reduce_scatter | solution.py:41
  212.3 13.3 %all-gather.3 = bf16[1,256,768]{2,1,0:T(8,128)(2,1)} all-gather(bf16[1,64,768]{2,1,0:T(8,128)(2,1)S(1)} %get-tuple-element.25), channel_id=5, replica_groups=mesh['ra_0'=8,'ra_1'=4,'cb'=8] {'ra_1'}, dimensions={1}, use_global_device_ids=true | all-gather | bytes 491520 | tf_op jit(solution)/shard_map/all_gather | solution.py:30
  225.7 14.2 %all-gather.19.cloned.1.call-done = bf16[512,2048]{1,0:T(8,128)(2,1)} async-done(((bf16[64,2048]{1,0:T(8,128)(2,1)}), bf16[512,2048]{1,0:T(8,128)(2,1)}) %all-gather.19.cloned.1.call-update) | async-done | bytes 2097168 | tf_op jit(solution)/shard_map/all_gather | solution.py:44
  242.4 3.6 collective-permute-start.1
  248.8 80.9 %all-gather.15.cloned.1.call-done = bf16[2048,1536]{1,0:T(8,128)(2,1)} async-done(((bf16[64,1536]{1,0:T(8,128)(2,1)}), bf16[2048,1536]{1,0:T(8,128)(2,1)}) %all-gather.15.cloned.1.call-update) | async-done | bytes 6291472 | tf_op jit(solution)/shard_map/all_gather | solution.py:24
  329.7 5.8 %multiply_multiply_fusion.1 = f32[514,768]{1,0:T(8,128)} fusion(bf16[2048,1536]{1,0:T(8,128)(2,1)} %all-gather.15.cloned.1.call-done, f32[2048]{0:T(1024)S(1)} %bitcast.104, f32[768]{0:T(1024)S(1)} %get-tuple-element.17, f32[514]{0:T(1024)S(1)} %add_rsqrt_fusion, bf16[512,2048]{1,0:T(8,128)(2,1)} %copy-done, bf16[2,2048]{1,0:T(2,128)(2,1)S(1)} %collective-permute-done.1), kind=kOutput, calls=%fused_computation.32 | convolution fusion | flops 1624009728 | bytes 6843400 | tf_op jit(solution)/shard_map/dot_general | solution.py:86
  335.5 3.1 multiply_multiply_fusion
  338.6 36.0 %all-gather.21.cloned.1.call-done = bf16[1,2048,768]{2,1,0:T(8,128)(2,1)} async-done(((bf16[1,256,768]{2,1,0:T(8,128)(2,1)}), bf16[1,2048,768]{2,1,0:T(8,128)(2,1)}) %all-gather.21.cloned.1.call-update) | async-done | bytes 3145744 | tf_op jit(solution)/shard_map/all_gather | solution.py:30
  374.6 8.9 %fusion.23 = bf16[512,2048]{1,0:T(8,128)(2,1)} fusion(bf16[1,2048,768]{2,1,0:T(8,128)(2,1)} %all-gather.21.cloned.1.call-done, f32[514,768]{1,0:T(8,128)} %multiply_multiply_fusion, f32[514,768]{1,0:T(8,128)} %multiply_multiply_fusion.1, f32[768]{0:T(1024)S(1)} %get-tuple-element.15, f32[768]{0:T(1024)S(1)} %get-tuple-element.16, ...), kind=kOutput, calls=%fused_computation.27 | convolution fusion | flops 1617952768 | bytes 14698496 | tf_op jit(solution)/shard_map/dot_general | solution.py:92
  383.5 35.1 %reduce-scatter.5.cloned.1.call-done = bf16[64,2048]{1,0:T(8,128)(2,1)} async-done(((bf16[512,2048]{1,0:T(8,128)(2,1)}), bf16[64,2048]{1,0:T(8,128)(2,1)}) %reduce-scatter.5.cloned.1.call-update) | async-done | bytes 262160 | tf_op jit(solution)/shard_map/reduce_scatter | solution.py:41
  418.6 28.6 %all-gather.23.cloned.1.call-done = bf16[512,2048]{1,0:T(8,128)(2,1)} async-done(((bf16[64,2048]{1,0:T(8,128)(2,1)}), bf16[512,2048]{1,0:T(8,128)(2,1)}) %all-gather.23.cloned.1.call-update) | async-done | bytes 2097168 | tf_op jit(solution)/shard_map/all_gather | solution.py:44
  447.2 3.8 fusion.26
  451.0 2.9 copy.16
  453.9 60.9 %all_to_all.24 = bf16[32,64,512]{2,1,0:T(8,128)(2,1)S(1)} all-to-all(bf16[32,64,512]{2,1,0:T(8,128)(2,1)S(1)} %bitcast.100), channel_id=1, replica_groups=mesh['ra_0'=8,'ra_1'=4,'cb'=8] {'ra_0','ra_1'}, dimensions={0} | all-to-all | bytes 4194304 | tf_op jit(solution)/shard_map/all_to_all | solution.py:102
  (96 shorter events, 35.1 us)
Async XLA Ops:
  6.5 3.0 copy-start.3
  6.5 115.2 %all-gather.13.cloned.1.call-start = ((), (), s32[]{:S(2)}) async-start(), calls=%async_computation.4 | async-start | bytes 6488064 | tf_op jit(solution)/shard_map/all_gather | solution.py:24
  29.8 11.9 %copy-start.4 = (f32[2,64,768]{2,1,0:T(8,128)S(1)}, f32[2,64,768]{2,1,0:T(8,128)}, u32[]{:S(2)}) copy-start(f32[2,64,768]{2,1,0:T(8,128)} %param.18) | copy-start | bytes 1179652
  29.8 26.6 %copy-start.9 = (f32[2,768]{1,0:T(2,128)S(1)}, f32[2,768]{1,0:T(2,128)}, u32[]{:S(2)}) copy-start(f32[2,768]{1,0:T(2,128)} %param.15) | copy-start | bytes 18436
  29.8 26.7 %copy-start.5 = (f32[2,3,768]{2,0,1:T(2,128)S(1)}, f32[2,3,768]{2,0,1:T(2,128)}, u32[]{:S(2)}) copy-start(f32[2,3,768]{2,0,1:T(2,128)} %param.16) | copy-start | bytes 55300
  29.8 26.7 %copy-start.6 = (f32[2,3,768]{2,0,1:T(2,128)S(1)}, f32[2,3,768]{2,0,1:T(2,128)}, u32[]{:S(2)}) copy-start(f32[2,3,768]{2,0,1:T(2,128)} %param.17) | copy-start | bytes 55300
  29.8 26.8 %copy-start.7 = (f32[2,2048]{1,0:T(2,128)S(1)}, f32[2,2048]{1,0:T(2,128)}, u32[]{:S(2)}) copy-start(f32[2,2048]{1,0:T(2,128)} %param.11) | copy-start | bytes 49156
  29.8 74.9 %all-to-all-start = ((bf16[32,64,512]{2,1,0:T(8,128)(2,1)}), bf16[32,64,512]{2,1,0:T(8,128)(2,1)S(1)}, u32[]{:S(2)}, u32[]{:S(2)}) async-start(bf16[32,64,512]{2,1,0:T(8,128)(2,1)} %constant_dynamic-update-slice_fusion), calls=%async_computation | async-start | bytes 4194304 | tf_op jit(solution)/shard_map/all_to_all | solution.py:70
  41.7 125.7 %all-gather.17.cloned.1.call-start = ((), (), s32[]{:S(2)}) async-start(), calls=%async_computation.8 | async-start | bytes 3538944 | tf_op jit(solution)/shard_map/all_gather | solution.py:30
  56.4 155.1 %reduce-scatter.3.cloned.1.call-start = ((), (), s32[]{:S(2)}) async-start(), calls=%async_computation.5 | async-start | bytes 2359296 | tf_op jit(solution)/shard_map/reduce_scatter | solution.py:41
  104.8 1.3 copy-start.2
  106.1 6.9 %copy-start.10 = (f32[2,768]{1,0:T(2,128)S(1)}, f32[2,768]{1,0:T(2,128)}, u32[]{:S(2)}) copy-start(f32[2,768]{1,0:T(2,128)} %param.14) | copy-start | bytes 18436
  109.1 5.5 %collective-permute-start = (bf16[2,2048]{1,0:T(2,128)(2,1)S(1)}, bf16[2,2048]{1,0:T(2,128)(2,1)S(1)}, u32[]{:S(2)}, u32[]{:S(2)}) collective-permute-start(bf16[2,2048]{1,0:T(2,128)(2,1)S(1)} %slice.194), channel_id=1, source_target_pairs={{0,8},{8,16},{16,24},{24,32},{32,40},{40,48},{48,56},{56,64},{64,7... | collective-permute-start | bytes 24584 | tf_op jit(solution)/shard_map/ppermute | solution.py:15
  121.7 5.2 copy-start.11
  176.3 49.4 %copy-start.8 = (f32[2,2048]{1,0:T(2,128)S(1)}, f32[2,2048]{1,0:T(2,128)}, u32[]{:S(2)}) copy-start(f32[2,2048]{1,0:T(2,128)} %param.19) | copy-start | bytes 49156
  176.4 63.6 %all-gather.19.cloned.1.call-start = ((), (), s32[]{:S(2)}) async-start(), calls=%async_computation.9 | async-start | bytes 2359296 | tf_op jit(solution)/shard_map/all_gather | solution.py:44
  211.5 118.2 %all-gather.15.cloned.1.call-start = ((), (), s32[]{:S(2)}) async-start(), calls=%async_computation.6 | async-start | bytes 6488064 | tf_op jit(solution)/shard_map/all_gather | solution.py:24
  212.3 162.3 %all-gather.21.cloned.1.call-start = ((), (), s32[]{:S(2)}) async-start(), calls=%async_computation.10 | async-start | bytes 3538944 | tf_op jit(solution)/shard_map/all_gather | solution.py:30
  225.6 193.0 %reduce-scatter.5.cloned.1.call-start = ((), (), s32[]{:S(2)}) async-start(), calls=%async_computation.7 | async-start | bytes 2359296 | tf_op jit(solution)/shard_map/reduce_scatter | solution.py:41
  242.4 5.6 %copy-start = (bf16[512,2048]{1,0:T(8,128)(2,1)}, bf16[512,2048]{1,0:T(8,128)(2,1)S(1)}, u32[]{:S(2)}) copy-start(bf16[512,2048]{1,0:T(8,128)(2,1)S(1)} %fusion.7) | copy-start | bytes 6291460
  242.4 5.5 %collective-permute-start.1 = (bf16[2,2048]{1,0:T(2,128)(2,1)S(1)}, bf16[2,2048]{1,0:T(2,128)(2,1)S(1)}, u32[]{:S(2)}, u32[]{:S(2)}) collective-permute-start(bf16[2,2048]{1,0:T(2,128)(2,1)S(1)} %slice.204), channel_id=1, source_target_pairs={{0,8},{8,16},{16,24},{24,32},{32,40},{40,48},{48,56},{56,64},{64,7... | collective-permute-start | bytes 24584 | tf_op jit(solution)/shard_map/ppermute | solution.py:15
  329.7 5.8 %copy-start.1 = (bf16[512,2048]{1,0:T(8,128)(2,1)S(1)}, bf16[512,2048]{1,0:T(8,128)(2,1)}, u32[]{:S(2)}) copy-start(bf16[512,2048]{1,0:T(8,128)(2,1)} %copy-done) | copy-start | bytes 6291460
  329.7 5.8 %copy-start.12 = (bf16[2048,1536]{1,0:T(8,128)(2,1)S(1)}, bf16[2048,1536]{1,0:T(8,128)(2,1)}, u32[]{:S(2)}) copy-start(bf16[2048,1536]{1,0:T(8,128)(2,1)} %all-gather.15.cloned.1.call-done) | copy-start | bytes 18874372
  383.5 63.7 %all-gather.23.cloned.1.call-start = ((), (), s32[]{:S(2)}) async-start(), calls=%async_computation.11 | async-start | bytes 2359296 | tf_op jit(solution)/shard_map/all_gather | solution.py:44
Sparse Core Ops, SparseCore 0:
  9.9 111.7 all-gather.12
  123.5 43.8 all-gather.16
  176.5 34.9 reduce-scatter.2
  213.2 26.6 all-gather.18
  242.3 87.3 all-gather.14
  331.4 43.1 all-gather.20
  383.6 34.9 reduce-scatter.4
  420.5 26.6 all-gather.22
